TPU v7x, 256 devices: a 2x2x32 block of a 4x8x32 slice. The times are simulated.
256 devices in a mesh: grp: 4 (over y, x), ep: 64 (over z, core).
Axes of the slice: x: 2, y: 2, z: 32, core: 2. Of those that a mesh axis runs over, the one named last changes fastest.
The devices are a block of a 4x8x32 slice.
Arguments:
- tokens: bfloat16 [1024, 2048], P(('grp', 'ep')), parts along dimension 0, may hold values from -6 to 6
- prior_state: float32 [1024, 32, 64, 64], P(('grp', 'ep')), parts along dimension 0, may hold values from -3 to 3
- receptance_matrix: bfloat16 [2048, 2048], P('ep'), may hold values from -0.125 to 0.125
- key_matrix: bfloat16 [2048, 2048], P('ep'), may hold values from -0.125 to 0.125
- value_matrix: bfloat16 [2048, 2048], P('ep'), may hold values from -0.125 to 0.125
- decay_lowrank_first: bfloat16 [2048, 64], replicated, may hold values from -0.125 to 0.125
- decay_lowrank_second: bfloat16 [64, 2048], replicated, may hold values from -1.5 to 1.5
- decay_channel_offset: float32 [2048], replicated, may hold values from -6 to 0
- correction_lowrank_first: bfloat16 [2048, 64], replicated, may hold values from -0.125 to 0.125
- correction_lowrank_second: bfloat16 [64, 2048], replicated, may hold values from -1.5 to 1.5
- correction_offset: float32 [2048], replicated, may hold values from -4 to 4
- gate_lowrank_first: bfloat16 [2048, 128], replicated, may hold values from -0.25 to 0.25
- gate_lowrank_second: bfloat16 [128, 2048], replicated, may hold values from -0.5 to 0.5
- key_rate_blend: float32 [2048], replicated, may hold values from 0.1 to 1.9
- self_token_scale: float32 [32, 64], replicated, may hold values from -1.2 to 1.2
- per_head_gain: float32 [2048], replicated, may hold values from 0.1 to 1.9
- per_head_bias: float32 [2048], replicated, may hold values from -1.8 to 1.8
- mixer_output_weight: bfloat16 [2048, 2048], P('ep'), may hold values from -0.125 to 0.125
- mixer_norm_gain: float32 [2048], replicated, may hold values from 0.1 to 1.9
- mixer_norm_bias: float32 [2048], replicated, may hold values from -1.8 to 1.8
- expert_norm_gain: float32 [2048], replicated, may hold values from 0.1 to 1.9
- expert_norm_bias: float32 [2048], replicated, may hold values from -1.8 to 1.8
- routes: int32 [1024, 4], P(('grp', 'ep')), parts along dimension 0, may hold values from 0 to 63, all different within a row; in each aligned block of 4 rows (0 to 3, 4 to 7, ...) at most 2 rows name the same one
- routing_weight: float32 [1024, 4], P(('grp', 'ep')), parts along dimension 0, may hold values from 0.1 to 1
- expert_gate_weight: bfloat16 [64, 2048, 512], P('ep'), may hold values from -0.125 to 0.125
- expert_up_weight: bfloat16 [64, 2048, 512], P('ep'), may hold values from -0.125 to 0.125
- expert_down_weight: bfloat16 [64, 512, 2048], P('ep'), may hold values from -0.25 to 0.25
Outputs:
- result: bfloat16 [1024, 2048], P(('grp', 'ep')), parts along dimension 0
- next_state: float32 [1024, 32, 64, 64], P(('grp', 'ep')), parts along dimension 0
There are 4 independent parts, one for each index of `grp`. A program takes and returns all parts, laid end to end along the dimension named above; an argument that names none is the same for every part. Nothing has to cross between parts.
Inputs may be any that keep to these rules, and one draw needn't show every extreme that they name: `routes`: A row names 4 different experts. Among the rows of one device no expert is named more than 2 times, and in some device one expert is named exactly 2 times; every expert is named somewhere.
All inputs are finite; a program needn't handle non-finite values.
Results may differ from a plain program's by a relative error of at most 0.0081.
Values may be sent and summed in bfloat16 or wider, within the bound.
No kernel may reach another device: no remote copies, remote signals or barrier semaphores. Data moves between devices by JAX's collectives and lax.ppermute only.
A program may use at most 128 MiB of HBM per device.

v0:
```python
import jax
import jax.numpy as jnp
from jax import lax
from jax.sharding import PartitionSpec as P


def side_by_side(arrays, axis, dim, along):
    widths = [a.shape[along] for a in arrays]
    both = jnp.concatenate(arrays, axis=along)
    whole = lax.all_gather(both, axis, axis=dim, tiled=True)
    return tuple(jnp.split(whole, [sum(widths[:k]) for k in range(1, len(widths))], axis=along))


def cut_along(value, dim, devices):
    shape = value.shape
    parts = value.reshape(*shape[:dim], devices, shape[dim] // devices, *shape[dim + 1 :])
    return jnp.moveaxis(parts, dim, 0)


def summed_on_arrival(value, axis, dim):
    devices = lax.axis_size(axis)
    parts = lax.all_to_all(cut_along(value, dim, devices), axis, 0, 0, tiled=True)
    return jnp.sum(parts.astype(jnp.float32), axis=0)


def layer_norm(values_in, gain_vec, bias_vec):
    row_mean = jnp.mean(values_in, -1, keepdims=True)
    centered = values_in - row_mean
    row_var = jnp.mean(centered * centered, -1, keepdims=True)
    return centered * lax.rsqrt(row_var + 1e-05) * gain_vec + bias_vec


def recurrent_readout(
    tokens,
    prior_state,
    receptance_rows,
    key_rows,
    value_rows,
    decay_lowrank_first,
    decay_lowrank_second,
    decay_channel_offset,
    correction_lowrank_first,
    correction_lowrank_second,
    correction_offset,
    gate_lowrank_first,
    gate_lowrank_second,
    key_rate_blend,
    self_token_scale,
    per_head_gain,
    per_head_bias,
):
    row_count = tokens.shape[0]
    head_count = prior_state.shape[1]
    head_size = prior_state.shape[2]
    squash = jnp.tanh(
        jnp.dot(tokens, decay_lowrank_first, preferred_element_type=jnp.float32)
    ).astype(jnp.bfloat16)
    pre_decay = decay_channel_offset + jnp.dot(
        squash, decay_lowrank_second, preferred_element_type=jnp.float32
    )
    decay_rate = jnp.exp(-jnp.exp(-jax.nn.softplus(-pre_decay) - 0.5))
    low_learn = jnp.dot(
        tokens, correction_lowrank_first, preferred_element_type=jnp.float32
    ).astype(jnp.bfloat16)
    learn_rate = jax.nn.sigmoid(
        correction_offset
        + jnp.dot(low_learn, correction_lowrank_second, preferred_element_type=jnp.float32)
    )
    opened = jax.nn.sigmoid(
        jnp.dot(tokens, gate_lowrank_first, preferred_element_type=jnp.float32)
    ).astype(jnp.bfloat16)
    gating = jnp.dot(opened, gate_lowrank_second, preferred_element_type=jnp.float32)

    def by_head(flat_arr):
        return flat_arr.reshape(row_count, head_count, head_size)

    scaled = by_head(key_rows)
    unit_key = scaled * lax.rsqrt(jnp.sum(scaled * scaled, -1, keepdims=True) + 1e-06)
    written_key = by_head(key_rows * (1.0 + (learn_rate - 1.0) * key_rate_blend))
    receptance_by_head = by_head(receptance_rows)
    value_by_head = by_head(value_rows)
    removed = jnp.einsum("nhvk,nhk->nhv", prior_state, unit_key, precision=lax.Precision.HIGHEST)
    next_state = (
        prior_state * by_head(decay_rate)[:, :, None, :]
        - removed[..., None] * (unit_key * by_head(learn_rate))[:, :, None, :]
        + value_by_head[..., None] * written_key[:, :, None, :]
    )
    readout = jnp.einsum(
        "nhvk,nhk->nhv", next_state, receptance_by_head, precision=lax.Precision.HIGHEST
    )
    head_mean = jnp.mean(readout, -1, keepdims=True)
    head_dev = readout - head_mean
    head_var = jnp.mean(head_dev * head_dev, -1, keepdims=True)
    normed = (head_dev * lax.rsqrt(head_var + 0.00064)).reshape(
        row_count, -1
    ) * per_head_gain + per_head_bias
    self_token_term = (
        jnp.sum(receptance_by_head * written_key * self_token_scale, -1, keepdims=True)
        * value_by_head
    )
    mixer_result = ((normed + self_token_term.reshape(row_count, -1)) * gating).astype(jnp.bfloat16)
    return (mixer_result, next_state)


def body(
    tokens,
    prior_state,
    receptance_matrix,
    key_matrix,
    value_matrix,
    decay_lowrank_first,
    decay_lowrank_second,
    decay_channel_offset,
    correction_lowrank_first,
    correction_lowrank_second,
    correction_offset,
    gate_lowrank_first,
    gate_lowrank_second,
    key_rate_blend,
    self_token_scale,
    per_head_gain,
    per_head_bias,
    mixer_output_weight,
    mixer_norm_gain,
    mixer_norm_bias,
    expert_norm_gain,
    expert_norm_bias,
    routes,
    routing_weight,
    expert_gate_weight,
    expert_up_weight,
    expert_down_weight,
):
    own_rows = tokens.shape[0]
    shard_rows = side_by_side((receptance_matrix, key_matrix, value_matrix), "ep", 0, 1)
    segment = tokens
    receptance_rows, key_rows, value_rows = tuple(
        (
            jnp.dot(segment, weight_mat, preferred_element_type=jnp.float32)
            for weight_mat in shard_rows
        )
    )
    mixer_result, next_state = recurrent_readout(
        tokens,
        prior_state,
        receptance_rows,
        key_rows,
        value_rows,
        decay_lowrank_first,
        decay_lowrank_second,
        decay_channel_offset,
        correction_lowrank_first,
        correction_lowrank_second,
        correction_offset,
        gate_lowrank_first,
        gate_lowrank_second,
        key_rate_blend,
        self_token_scale,
        per_head_gain,
        per_head_bias,
    )
    mixer_cols = lax.all_to_all(mixer_result, "ep", split_axis=1, concat_axis=0, tiled=True)
    segment = mixer_cols
    mixed = summed_on_arrival(
        jnp.dot(segment, mixer_output_weight, preferred_element_type=jnp.float32).astype(
            jnp.bfloat16
        ),
        "ep",
        0,
    )
    hidden = layer_norm(
        tokens.astype(jnp.float32) + mixed, mixer_norm_gain, mixer_norm_bias
    ).astype(jnp.bfloat16)
    model_width = hidden.shape[1]
    top_count = routes.shape[1]
    expert_count = lax.axis_size("ep")
    capacity = max(2, 2 * own_rows * top_count // expert_count)
    flat_ids = routes.reshape(-1)
    onehot = (flat_ids[:, None] == jnp.arange(expert_count, dtype=jnp.int32)[None, :]).astype(
        jnp.int32
    )
    earlier = jnp.cumsum(onehot, 0) - onehot
    slot_rank = jnp.sum(earlier * onehot, 1)
    target = flat_ids * capacity + slot_rank
    dispatch = (
        target[:, None] == jnp.arange(expert_count * capacity, dtype=jnp.int32)[None, :]
    ).astype(jnp.bfloat16)
    repeated = jnp.repeat(hidden, top_count, axis=0)
    outgoing = lax.dot_general(
        dispatch, repeated, (((0,), (0,)), ((), ())), preferred_element_type=jnp.float32
    ).astype(jnp.bfloat16)
    outgoing = outgoing.reshape(expert_count, capacity, model_width)
    arrived = lax.all_to_all(outgoing, "ep", split_axis=0, concat_axis=0, tiled=True)
    sources, slot_count, width_in = arrived.shape
    flat_in = arrived.reshape(sources * slot_count, width_in)
    gate_val = jnp.dot(flat_in, expert_gate_weight[0], preferred_element_type=jnp.float32)
    up_val = jnp.dot(flat_in, expert_up_weight[0], preferred_element_type=jnp.float32)
    inner = (jax.nn.silu(gate_val) * up_val).astype(jnp.bfloat16)
    produced = jnp.dot(inner, expert_down_weight[0], preferred_element_type=jnp.float32).astype(
        jnp.bfloat16
    )
    returned = lax.all_to_all(
        produced.reshape(sources, slot_count, width_in),
        "ep",
        split_axis=0,
        concat_axis=0,
        tiled=True,
    )
    picked = jnp.dot(
        dispatch,
        returned.reshape(expert_count * capacity, model_width),
        preferred_element_type=jnp.float32,
    )
    share = routing_weight / jnp.sum(routing_weight, -1, keepdims=True)
    combined = jnp.sum(picked.reshape(own_rows, top_count, model_width) * share[..., None], 1)
    result = layer_norm(
        hidden.astype(jnp.float32) + combined, expert_norm_gain, expert_norm_bias
    ).astype(jnp.bfloat16)
    return (result, next_state)


def solution(mesh):
    in_specs = (
        P(("grp", "ep"), None),
        P(("grp", "ep"), None, None, None),
        P("ep", None),
        P("ep", None),
        P("ep", None),
        P(),
        P(),
        P(),
        P(),
        P(),
        P(),
        P(),
        P(),
        P(),
        P(),
        P(),
        P(),
        P("ep", None),
        P(),
        P(),
        P(),
        P(),
        P(("grp", "ep"), None),
        P(("grp", "ep"), None),
        P("ep", None, None),
        P("ep", None, None),
        P("ep", None, None),
    )
    out_specs = (P(("grp", "ep"), None), P(("grp", "ep"), None, None, None))
    return jax.shard_map(body, mesh=mesh, in_specs=in_specs, out_specs=out_specs, check_vma=False)
```

profile of v0, /device:TPU:38, one launch (start us, length us, event | category | flops | bytes accessed | tf_op | source)
XLA Modules:
  0.0 540.0 jit_solution(7225675819815774377)
XLA Ops:
  7.3 1.9 pad_maximum_fusion
  9.3 1.4 fusion.19
  10.8 1.5 fusion.52
  12.4 172.6 %all-gather.2.cloned.1.call-done = bf16[2048,6144]{1,0:T(8,128)(2,1)} async-done(((bf16[32,6144]{1,0:T(8,128)(2,1)}), bf16[2048,6144]{1,0:T(8,128)(2,1)}) %all-gather.2.cloned.1.call-update) | async-done | bytes 25165840 | tf_op jit(solution)/shard_map/all_gather | solution.py:10
  185.0 4.6 fusion.13
  189.8 4.6 add_multiply_fusion
  194.7 4.6 fusion.10
  199.7 8.7 %fusion.66 = f32[4,32,1,64]{3,2,1,0:T(1,128)S(1)} fusion(f32[4,32,64,1]{2,3,1,0:T(1,128)S(1)} %bitcast.62, f32[4,32,64,64]{3,2,1,0:T(8,128)} %param.28), kind=kOutput, calls=%fused_computation.93 | convolution fusion | flops 6291456 | bytes 2162688 | tf_op jit(solution)/shard_map/nhvk,nhk->nhv/dot_general | solution.py:82
  208.4 2.8 multiply_add_fusion
  211.2 2.0 copy-done.2
  213.2 6.6 %fusion.67 = f32[4,32,1,64]{3,2,1,0:T(1,128)S(1)} fusion(f32[4,32,64,64]{3,2,1,0:T(8,128)S(1)} %multiply_add_fusion, f32[4,32,64,1]{2,3,1,0:T(1,128)S(1)} %bitcast.61), kind=kOutput, calls=%fused_computation.94 | convolution fusion | flops 6291456 | bytes 2162688 | tf_op jit(solution)/shard_map/nhvk,nhk->nhv/dot_general | solution.py:88
  220.3 1.4 fusion.21
  221.9 42.3 %all_to_all.34 = bf16[4,64,32]{2,0,1:T(4,128)(2,1)S(1)} all-to-all(bf16[4,64,32]{2,0,1:T(4,128)(2,1)S(1)} %copy.30), channel_id=1, replica_groups=mesh['grp'=4,'ep'=64] {'ep'}, dimensions={1} | all-to-all | bytes 32768 | tf_op jit(solution)/shard_map/all_to_all | solution.py:162
  264.2 0.4 convolution_convert_fusion
  264.6 1.2 reshape.149
  265.8 6.7 %all-to-all-start.1 = ((bf16[64,4,2048]{2,1,0:T(4,128)(2,1)}), bf16[64,4,2048]{2,1,0:T(4,128)(2,1)S(1)}, u32[]{:S(2)}, u32[]{:S(2)}) async-start(bf16[64,4,2048]{2,1,0:T(4,128)(2,1)} %reshape.149), calls=%async_computation.1 | async-start | bytes 2097152 | tf_op jit(solution)/shard_map/all_to_all | solution.py:22
  273.0 108.6 %all-to-all-done.1 = bf16[64,4,2048]{2,1,0:T(4,128)(2,1)S(1)} async-done(((bf16[64,4,2048]{2,1,0:T(4,128)(2,1)}), bf16[64,4,2048]{2,1,0:T(4,128)(2,1)S(1)}, u32[]{:S(2)}, u32[]{:S(2)}) %all-to-all-start.1) | async-done | bytes 1048608 | tf_op jit(solution)/shard_map/all_to_all | solution.py:22
  381.6 0.4 convert_reduce_fusion
  382.2 0.2 multiply_reduce_fusion.4
  382.6 0.4 convolution_convert_fusion.2
  383.0 0.3 reshape.151
  383.3 70.6 %all_to_all.35 = bf16[64,2,2048]{2,1,0:T(2,128)(2,1)} all-to-all(bf16[64,2,2048]{2,1,0:T(2,128)(2,1)S(1)} %reshape.151), channel_id=1, replica_groups=mesh['grp'=4,'ep'=64] {'ep'}, dimensions={0} | all-to-all | bytes 1048576 | tf_op jit(solution)/shard_map/all_to_all | solution.py:193
  453.9 1.2 reshape.152
  455.2 2.0 fusion.25
  457.3 2.4 convolution_convert_fusion.1
  459.7 1.1 reshape.153
  460.8 6.5 %all-to-all-start.3 = ((bf16[64,2,2048]{2,1,0:T(2,128)(2,1)}), bf16[64,2,2048]{2,1,0:T(2,128)(2,1)S(1)}, u32[]{:S(2)}, u32[]{:S(2)}) async-start(bf16[64,2,2048]{2,1,0:T(2,128)(2,1)} %reshape.153), calls=%async_computation.3 | async-start | bytes 1048576 | tf_op jit(solution)/shard_map/all_to_all | solution.py:202
  467.6 64.0 %all-to-all-done.3 = bf16[64,2,2048]{2,1,0:T(2,128)(2,1)S(1)} async-done(((bf16[64,2,2048]{2,1,0:T(2,128)(2,1)}), bf16[64,2,2048]{2,1,0:T(2,128)(2,1)S(1)}, u32[]{:S(2)}, u32[]{:S(2)}) %all-to-all-start.3) | async-done | bytes 524320 | tf_op jit(solution)/shard_map/all_to_all | solution.py:202
  531.6 0.2 reshape.159
  531.8 0.3 fusion.35
  532.2 0.2 multiply_reduce_fusion.3
  532.4 0.7 add_convert_fusion
  (71 shorter events, 3.0 us)
Async XLA Ops:
  7.2 450.0 %copy-start = (bf16[1,512,2048]{2,1,0:T(8,128)(2,1)S(1)}, bf16[1,512,2048]{2,1,0:T(8,128)(2,1)}, u32[]{:S(2)}) copy-start(bf16[1,512,2048]{2,1,0:T(8,128)(2,1)} %param.53) | copy-start | bytes 6291460
  7.2 177.8 %all-gather.2.cloned.1.call-start = ((), (), s32[]{:S(2)}) async-start(), calls=%async_computation.4 | async-start | bytes 25559040 | tf_op jit(solution)/shard_map/all_gather | solution.py:10
  12.4 177.4 %copy-start.3 = (bf16[4,2048]{1,0:T(4,128)(2,1)S(1)}, bf16[4,2048]{1,0:T(4,128)(2,1)}, u32[]{:S(2)}) copy-start(bf16[4,2048]{1,0:T(4,128)(2,1)} %param.27) | copy-start | bytes 49156
  12.4 177.4 %copy-start.15 = (f32[2048]{0:T(1024)S(1)}, f32[2048]{0:T(1024)}, u32[]{:S(2)}) copy-start(f32[2048]{0:T(1024)} %param.40) | copy-start | bytes 24580
  189.8 4.7 copy-start.6
  199.5 8.9 %copy-start.1 = (f32[4,32,64,64]{3,2,1,0:T(8,128)S(1)}, f32[4,32,64,64]{3,2,1,0:T(8,128)}, u32[]{:S(2)}) copy-start(f32[4,32,64,64]{3,2,1,0:T(8,128)} %param.28) | copy-start | bytes 6291460
  211.2 2.0 copy-start.2
  211.2 9.1 %copy-start.4 = (bf16[128,2048]{1,0:T(8,128)(2,1)S(1)}, bf16[128,2048]{1,0:T(8,128)(2,1)}, u32[]{:S(2)}) copy-start(bf16[128,2048]{1,0:T(8,128)(2,1)} %param.39) | copy-start | bytes 1572868
  211.2 9.1 %copy-start.7 = (f32[2048]{0:T(1024)S(1)}, f32[2048]{0:T(1024)}, u32[]{:S(2)}) copy-start(f32[2048]{0:T(1024)} %param.43) | copy-start | bytes 24580
  211.2 9.1 %copy-start.8 = (f32[2048]{0:T(1024)S(1)}, f32[2048]{0:T(1024)}, u32[]{:S(2)}) copy-start(f32[2048]{0:T(1024)} %param.42) | copy-start | bytes 24580
  211.2 53.0 %copy-start.5 = (bf16[32,2048]{1,0:T(8,128)(2,1)S(1)}, bf16[32,2048]{1,0:T(8,128)(2,1)}, u32[]{:S(2)}) copy-start(bf16[32,2048]{1,0:T(8,128)(2,1)} %param.44) | copy-start | bytes 393220
  219.8 52.8 %copy-start.9 = (s32[4,4]{1,0:T(4,128)S(1)}, s32[4,4]{1,0:T(4,128)}, u32[]{:S(2)}) copy-start(s32[4,4]{1,0:T(4,128)} %param.49) | copy-start | bytes 196
  220.1 162.3 %copy-start.11 = (f32[2048]{0:T(1024)S(1)}, f32[2048]{0:T(1024)}, u32[]{:S(2)}) copy-start(f32[2048]{0:T(1024)} %param.46) | copy-start | bytes 24580
  220.1 162.3 %copy-start.12 = (f32[2048]{0:T(1024)S(1)}, f32[2048]{0:T(1024)}, u32[]{:S(2)}) copy-start(f32[2048]{0:T(1024)} %param.45) | copy-start | bytes 24580
  265.8 115.8 %all-to-all-start.1 = ((bf16[64,4,2048]{2,1,0:T(4,128)(2,1)}), bf16[64,4,2048]{2,1,0:T(4,128)(2,1)S(1)}, u32[]{:S(2)}, u32[]{:S(2)}) async-start(bf16[64,4,2048]{2,1,0:T(4,128)(2,1)} %reshape.149), calls=%async_computation.1 | async-start | bytes 2097152 | tf_op jit(solution)/shard_map/all_to_all | solution.py:22
  457.2 10.2 %copy-start.10 = (f32[4,4]{1,0:T(4,128)S(1)}, f32[4,4]{1,0:T(4,128)}, u32[]{:S(2)}) copy-start(f32[4,4]{1,0:T(4,128)} %param.50) | copy-start | bytes 196
  457.2 75.2 %copy-start.13 = (f32[2048]{0:T(1024)S(1)}, f32[2048]{0:T(1024)}, u32[]{:S(2)}) copy-start(f32[2048]{0:T(1024)} %param.48) | copy-start | bytes 24580
  457.2 75.2 %copy-start.14 = (f32[2048]{0:T(1024)S(1)}, f32[2048]{0:T(1024)}, u32[]{:S(2)}) copy-start(f32[2048]{0:T(1024)} %param.47) | copy-start | bytes 24580
  460.8 70.7 %all-to-all-start.3 = ((bf16[64,2,2048]{2,1,0:T(2,128)(2,1)}), bf16[64,2,2048]{2,1,0:T(2,128)(2,1)S(1)}, u32[]{:S(2)}, u32[]{:S(2)}) async-start(bf16[64,2,2048]{2,1,0:T(2,128)(2,1)} %reshape.153), calls=%async_computation.3 | async-start | bytes 1048576 | tf_op jit(solution)/shard_map/all_to_all | solution.py:202
Sparse Core Ops, SparseCore 0:
  10.5 174.5 all-gather.1
where the time goes:
time: 541 us; the launch traced here: 540 us
  waiting for transfers between devices  345 us (64%)
  blocking collectives  113 us (21%)
  matrix products  38.9 us (7%)
  between operations  14.4 us (3%)
  starting transfers between devices  13.3 us (2%)
  other arithmetic  7.77 us (1%)
  local copies, waits for them, and re-layouts  7.44 us (1%)
    all_gather x1, waiting for transfers between devices, side_by_side(): whole = lax.all_gather(both, axis, axis=dim, tiled=True)  173 us
    all_to_all x1, waiting for transfers between devices, summed_on_arrival(): lax.all_to_all(cut_along(value, dim, devices), axis, 0, 0, tiled=True)  109 us
    all_to_all x1, blocking collectives, body(): lax.all_to_all(outgoing, 'ep', split_axis=0, concat_axis=0, tiled=True)  70.6 us
    all_to_all x1, waiting for transfers between devices, body(): lax.all_to_all(produced.reshape(sources, slot_count, width_in), 'ep', spl...  64 us
    all_to_all x1, blocking collectives, body(): lax.all_to_all(mixer_result, 'ep', split_axis=1, concat_axis=0, tiled=True)  42.3 us
    dot_general x3, matrix products, body(): jnp.dot(segment, weight_mat, preferred_element_type=jnp.float32)  13.7 us
  transfers between devices with their start and end apart: 3, of which 3 were waited for; matrix products, arithmetic and copies ran while one was open for 1% of the time, Pallas kernels for 0%

commit v1 on v0

--- a/solution.py
+++ b/solution.py
@@ -4,23 +4,31 @@
 from jax.sharding import PartitionSpec as P
 
 
-def side_by_side(arrays, axis, dim, along):
-    widths = [a.shape[along] for a in arrays]
-    both = jnp.concatenate(arrays, axis=along)
-    whole = lax.all_gather(both, axis, axis=dim, tiled=True)
-    return tuple(jnp.split(whole, [sum(widths[:k]) for k in range(1, len(widths))], axis=along))
-
-
-def cut_along(value, dim, devices):
-    shape = value.shape
-    parts = value.reshape(*shape[:dim], devices, shape[dim] // devices, *shape[dim + 1 :])
-    return jnp.moveaxis(parts, dim, 0)
-
-
-def summed_on_arrival(value, axis, dim):
+NEAR = 8
+
+
+def near_and_far(axis):
     devices = lax.axis_size(axis)
-    parts = lax.all_to_all(cut_along(value, dim, devices), axis, 0, 0, tiled=True)
-    return jnp.sum(parts.astype(jnp.float32), axis=0)
+    blocks = devices // NEAR
+    near = [[NEAR * b + j for j in range(NEAR)] for b in range(blocks)]
+    far = [[NEAR * b + j for b in range(blocks)] for j in range(NEAR)]
+    return near, far
+
+
+def swap_features(value, axis, far):
+    return lax.all_to_all(value, axis, split_axis=1, concat_axis=0, tiled=True, axis_index_groups=far)
+
+
+def added_on_arrival(parts, axis, groups):
+    got = lax.all_to_all(parts, axis, split_axis=0, concat_axis=0, tiled=True, axis_index_groups=groups)
+    return jnp.sum(got.astype(jnp.float32), axis=0)
+
+
+def spread_product(rows, weight, axis, far):
+    own_rows = rows.shape[0]
+    swapped = swap_features(rows, axis, far)
+    part = jnp.dot(swapped, weight, preferred_element_type=jnp.float32).astype(jnp.bfloat16)
+    return added_on_arrival(part.reshape(-1, own_rows, weight.shape[1]), axis, far)
 
 
 def layer_norm(values_in, gain_vec, bias_vec):
@@ -131,14 +139,16 @@
     expert_up_weight,
     expert_down_weight,
 ):
-    own_rows = tokens.shape[0]
-    shard_rows = side_by_side((receptance_matrix, key_matrix, value_matrix), "ep", 0, 1)
-    segment = tokens
-    receptance_rows, key_rows, value_rows = tuple(
-        (
-            jnp.dot(segment, weight_mat, preferred_element_type=jnp.float32)
-            for weight_mat in shard_rows
-        )
+    own_rows, model_width = tokens.shape
+    top_count = routes.shape[1]
+    near, far = near_and_far("ep")
+    mixer_weight = lax.all_gather(
+        jnp.concatenate((receptance_matrix, key_matrix, value_matrix), axis=1),
+        "ep", axis=0, tiled=True, axis_index_groups=near,
+    )
+    output_weight = lax.all_gather(mixer_output_weight, "ep", axis=0, tiled=True, axis_index_groups=near)
+    receptance_rows, key_rows, value_rows = jnp.split(
+        spread_product(tokens, mixer_weight, "ep", far), 3, axis=1
     )
     mixer_result, next_state = recurrent_readout(
         tokens,
@@ -159,60 +169,31 @@
         per_head_gain,
         per_head_bias,
     )
-    mixer_cols = lax.all_to_all(mixer_result, "ep", split_axis=1, concat_axis=0, tiled=True)
-    segment = mixer_cols
-    mixed = summed_on_arrival(
-        jnp.dot(segment, mixer_output_weight, preferred_element_type=jnp.float32).astype(
-            jnp.bfloat16
-        ),
-        "ep",
-        0,
-    )
+    mixed = spread_product(mixer_result, output_weight, "ep", far)
     hidden = layer_norm(
         tokens.astype(jnp.float32) + mixed, mixer_norm_gain, mixer_norm_bias
     ).astype(jnp.bfloat16)
-    model_width = hidden.shape[1]
-    top_count = routes.shape[1]
-    expert_count = lax.axis_size("ep")
-    capacity = max(2, 2 * own_rows * top_count // expert_count)
-    flat_ids = routes.reshape(-1)
-    onehot = (flat_ids[:, None] == jnp.arange(expert_count, dtype=jnp.int32)[None, :]).astype(
-        jnp.int32
-    )
-    earlier = jnp.cumsum(onehot, 0) - onehot
-    slot_rank = jnp.sum(earlier * onehot, 1)
-    target = flat_ids * capacity + slot_rank
-    dispatch = (
-        target[:, None] == jnp.arange(expert_count * capacity, dtype=jnp.int32)[None, :]
-    ).astype(jnp.bfloat16)
-    repeated = jnp.repeat(hidden, top_count, axis=0)
-    outgoing = lax.dot_general(
-        dispatch, repeated, (((0,), (0,)), ((), ())), preferred_element_type=jnp.float32
-    ).astype(jnp.bfloat16)
-    outgoing = outgoing.reshape(expert_count, capacity, model_width)
-    arrived = lax.all_to_all(outgoing, "ep", split_axis=0, concat_axis=0, tiled=True)
-    sources, slot_count, width_in = arrived.shape
-    flat_in = arrived.reshape(sources * slot_count, width_in)
-    gate_val = jnp.dot(flat_in, expert_gate_weight[0], preferred_element_type=jnp.float32)
-    up_val = jnp.dot(flat_in, expert_up_weight[0], preferred_element_type=jnp.float32)
+    share = routing_weight / jnp.sum(routing_weight, -1, keepdims=True)
+    share_high = lax.reduce_precision(share, 8, 7)
+    share_low = share - share_high
+    tail = jnp.concatenate((routes.astype(jnp.float32), share_high, share_low), axis=1)
+    tail = jnp.pad(tail.astype(jnp.bfloat16), ((0, 0), (0, 128 - tail.shape[1])))
+    gathered = lax.all_gather(
+        jnp.concatenate((hidden, tail), axis=1), "ep", axis=0, tiled=True
+    )
+    rows_in = gathered[:, :model_width]
+    tail_in = gathered[:, model_width:].astype(jnp.float32)
+    named = tail_in[:, :top_count] == lax.axis_index("ep").astype(jnp.float32)
+    shares = tail_in[:, top_count : 2 * top_count] + tail_in[:, 2 * top_count : 3 * top_count]
+    weight_of = jnp.sum(jnp.where(named, shares, 0.0), axis=1, keepdims=True)
+    gate_val = jnp.dot(rows_in, expert_gate_weight[0], preferred_element_type=jnp.float32)
+    up_val = jnp.dot(rows_in, expert_up_weight[0], preferred_element_type=jnp.float32)
     inner = (jax.nn.silu(gate_val) * up_val).astype(jnp.bfloat16)
-    produced = jnp.dot(inner, expert_down_weight[0], preferred_element_type=jnp.float32).astype(
-        jnp.bfloat16
-    )
-    returned = lax.all_to_all(
-        produced.reshape(sources, slot_count, width_in),
-        "ep",
-        split_axis=0,
-        concat_axis=0,
-        tiled=True,
-    )
-    picked = jnp.dot(
-        dispatch,
-        returned.reshape(expert_count * capacity, model_width),
-        preferred_element_type=jnp.float32,
-    )
-    share = routing_weight / jnp.sum(routing_weight, -1, keepdims=True)
-    combined = jnp.sum(picked.reshape(own_rows, top_count, model_width) * share[..., None], 1)
+    produced = jnp.dot(inner, expert_down_weight[0], preferred_element_type=jnp.float32)
+    given = (produced * weight_of).astype(jnp.bfloat16)
+    by_class = given.reshape(-1, NEAR, own_rows, model_width).swapaxes(0, 1)
+    block_sum = added_on_arrival(by_class, "ep", near).astype(jnp.bfloat16)
+    combined = added_on_arrival(block_sum, "ep", far)
     result = layer_norm(
         hidden.astype(jnp.float32) + combined, expert_norm_gain, expert_norm_bias
     ).astype(jnp.bfloat16)

time: 541 us -> 441 us (0.82)
  waiting for transfers between devices: 345 us -> 198 us
  blocking collectives: 113 us -> 158 us
  starting transfers between devices: 13.3 us -> 22.1 us
  matrix products: 38.9 us -> 30.5 us
    all_to_all x2, waiting for transfers between devices: 173 us -> 64.9 us  [added_on_arrival(): lax.all_to_all(parts, axis, split_axis=0, concat_axis=0, tiled=True, axis...]
    all_to_all x2 -> x4, blocking collectives: 113 us -> 158 us  [the longest x2 88.4 us: swap_features(): lax.all_to_all(value, axis, split_axis=1, concat_axis=0, tiled=True, axis...]
    all_gather x1 -> x3, waiting for transfers between devices: 173 us -> 132 us  [the longest x1 117 us: body(): lax.all_gather(jnp.concatenate((hidden, tail), axis=1), 'ep', axis=0, til...]
    dot_general x7 -> x3, matrix products: 16.9 us -> 7.18 us  [the longest x2 4.06 us: spread_product(): jnp.dot(swapped, weight, preferred_element_type=jnp.float32)]
    all_to_all x2, starting transfers between devices: 13.2 us -> 21.7 us  [added_on_arrival(): lax.all_to_all(parts, axis, split_axis=0, concat_axis=0, tiled=True, axis...]
  transfers between devices with their start and end apart: 3 -> 5, of which waited for: 3 -> 4; matrix products, arithmetic and copies ran while one was open for 1% -> 6% of each run, Pallas kernels for 0% -> 0%
where the time goes in v1:
time: 441 us; the launch traced here: 440 us
  waiting for transfers between devices  198 us (45%)
  blocking collectives  158 us (36%)
  matrix products  30.5 us (7%)
  starting transfers between devices  22.1 us (5%)
  between operations  14.1 us (3%)
  other arithmetic  9.61 us (2%)
  local copies, waits for them, and re-layouts  7.27 us (2%)
    all_gather x1, waiting for transfers between devices, body(): lax.all_gather(jnp.concatenate((hidden, tail), axis=1), 'ep', axis=0, til...  117 us
    all_to_all x2, blocking collectives, swap_features(): lax.all_to_all(value, axis, split_axis=1, concat_axis=0, tiled=True, axis...  88.4 us
    all_to_all x2, blocking collectives, added_on_arrival(): lax.all_to_all(parts, axis, split_axis=0, concat_axis=0, tiled=True, axis...  70.1 us
    all_to_all x2, waiting for transfers between devices, added_on_arrival(): lax.all_to_all(parts, axis, split_axis=0, concat_axis=0, tiled=True, axis...  64.9 us
    all_to_all x2, starting transfers between devices, added_on_arrival(): lax.all_to_all(parts, axis, split_axis=0, concat_axis=0, tiled=True, axis...  21.7 us
    all_gather x1, waiting for transfers between devices, body(): lax.all_gather(jnp.concatenate((receptance_matrix, key_matrix, value_matr...  15.5 us
  transfers between devices with their start and end apart: 5, of which 4 were waited for; matrix products, arithmetic and copies ran while one was open for 6% of the time, Pallas kernels for 0%

profile of v1, /device:TPU:38, one launch (start us, length us, event | category | flops | bytes accessed | tf_op | source)
XLA Modules:
  0.0 439.9 jit_solution(10776442208804594551)
XLA Ops:
  7.3 1.9 pad_maximum_fusion
  9.3 54.0 %all_to_all.58 = bf16[4,8,256]{2,0,1:T(4,128)(2,1)S(1)} all-to-all(bf16[4,8,256]{2,0,1:T(4,128)(2,1)} %bitcast.55), channel_id=1, replica_groups={{0,8,16,24,32,40,48,56},{1,9,17,25,33,41,49,57},{2,10,18,26,34,42,50,58..., dimensions={1} | all-to-all | bytes 32768 | tf_op jit(solution)/shard_map/all_to_all | solution.py:19
  63.2 0.6 all_to_all.43
  63.9 15.5 %all-gather.5.cloned.1.call-done = bf16[256,6144]{1,0:T(8,128)(2,1)} async-done(((bf16[32,6144]{1,0:T(8,128)(2,1)}), bf16[256,6144]{1,0:T(8,128)(2,1)}) %all-gather.5.cloned.1.call-update) | async-done | bytes 3145744 | tf_op jit(solution)/shard_map/all_gather | solution.py:145
  79.3 2.5 fusion.1
  81.9 0.9 reshape.104
  82.8 18.1 %all-to-all-start.1 = ((bf16[8,4,6144]{2,1,0:T(4,128)(2,1)}), bf16[8,4,6144]{2,1,0:T(4,128)(2,1)S(1)}, u32[]{:S(2)}, u32[]{:S(2)}) async-start(bf16[8,4,6144]{2,1,0:T(4,128)(2,1)} %reshape.104), calls=%async_computation.1 | async-start | bytes 786432 | tf_op jit(solution)/shard_map/all_to_all | solution.py:23
  101.0 0.7 all-gather.7.cloned.1.call-update
  101.7 1.7 fusion.43
  103.5 0.9 mul.170
  104.4 1.1 fusion.6
  105.6 38.6 %all-to-all-done.1 = bf16[8,4,6144]{2,1,0:T(4,128)(2,1)S(1)} async-done(((bf16[8,4,6144]{2,1,0:T(4,128)(2,1)}), bf16[8,4,6144]{2,1,0:T(4,128)(2,1)S(1)}, u32[]{:S(2)}, u32[]{:S(2)}) %all-to-all-start.1) | async-done | bytes 393248 | tf_op jit(solution)/shard_map/all_to_all | solution.py:23
  144.3 0.7 fusion.58
  145.9 8.5 %fusion.59 = f32[4,32,1,64]{3,2,1,0:T(1,128)S(1)} fusion(f32[4,32,64,1]{2,3,1,0:T(1,128)S(1)} %bitcast.58, f32[4,32,64,64]{3,2,1,0:T(8,128)} %param.28), kind=kOutput, calls=%fused_computation.96 | convolution fusion | flops 6291456 | bytes 2162688 | tf_op jit(solution)/shard_map/nhvk,nhk->nhv/dot_general | solution.py:90
  154.4 2.8 multiply_add_fusion
  157.3 6.6 %fusion.60 = f32[4,32,1,64]{3,2,1,0:T(1,128)S(1)} fusion(f32[4,32,64,64]{3,2,1,0:T(8,128)S(1)} %multiply_add_fusion, f32[4,32,64,1]{2,3,1,0:T(1,128)S(1)} %bitcast.57), kind=kOutput, calls=%fused_computation.97 | convolution fusion | flops 6291456 | bytes 2162688 | tf_op jit(solution)/shard_map/nhvk,nhk->nhv/dot_general | solution.py:96
  164.4 1.4 fusion.8
  165.8 34.5 %all_to_all.59 = bf16[4,8,256]{2,0,1:T(4,128)(2,1)S(1)} all-to-all(bf16[4,8,256]{2,0,1:T(4,128)(2,1)S(1)} %bitcast.59), channel_id=1, replica_groups={{0,8,16,24,32,40,48,56},{1,9,17,25,33,41,49,57},{2,10,18,26,34,42,50,58..., dimensions={1} | all-to-all | bytes 32768 | tf_op jit(solution)/shard_map/all_to_all | solution.py:19
  200.3 1.5 convolution_convert_fusion.1
  201.9 0.7 reshape.109
  202.6 3.6 all-to-all-start.3
  206.7 26.3 %all-to-all-done.3 = bf16[8,4,2048]{2,1,0:T(4,128)(2,1)S(1)} async-done(((bf16[8,4,2048]{2,1,0:T(4,128)(2,1)}), bf16[8,4,2048]{2,1,0:T(4,128)(2,1)S(1)}, u32[]{:S(2)}, u32[]{:S(2)}) %all-to-all-start.3) | async-done | bytes 131104 | tf_op jit(solution)/shard_map/all_to_all | solution.py:23
  233.5 0.6 maximum_bitcast_fusion
  234.2 116.6 %all-gather.9.cloned.1.call-done = bf16[64,4,2176]{2,1,0:T(4,128)(2,1)} async-done(((bf16[1,4,2176]{2,1,0:T(4,128)(2,1)}), bf16[64,4,2176]{2,1,0:T(4,128)(2,1)}) %all-gather.9.cloned.1.call-update) | async-done | bytes 1114128 | tf_op jit(solution)/shard_map/all_gather | solution.py:181
  350.8 1.4 reshape.112
  352.2 3.1 fusion.12
  355.5 4.0 fusion.2
  359.5 1.5 reshape.110
  361.5 29.1 %all_to_all.60 = bf16[8,8,4,2048]{3,2,1,0:T(4,128)(2,1)S(1)} all-to-all(bf16[8,8,4,2048]{3,2,1,0:T(4,128)(2,1)S(1)} %bitcast.51), channel_id=1, replica_groups={{0,1,2,3,4,5,6,7},{8,9,10,11,12,13,14,15},{16,17,18,19,20,21,22,23},{24..., dimensions={0} | all-to-all | bytes 2097152 | tf_op jit(solution)/shard_map/all_to_all | solution.py:23
  390.6 0.6 reduce_sum.139
  391.2 40.9 %all_to_all.61 = bf16[8,4,2048]{2,1,0:T(4,128)(2,1)S(1)} all-to-all(bf16[8,4,2048]{2,1,0:T(4,128)(2,1)S(1)} %reduce_sum.139), channel_id=1, replica_groups={{0,8,16,24,32,40,48,56},{1,9,17,25,33,41,49,57},{2,10,18,26,34,42,50,58..., dimensions={0} | all-to-all | bytes 262144 | tf_op jit(solution)/shard_map/all_to_all | solution.py:23
  432.7 0.7 add_convert_fusion
  (80 shorter events, 4.2 us)
Async XLA Ops:
  7.2 348.3 %copy-start = (bf16[1,512,2048]{2,1,0:T(8,128)(2,1)S(1)}, bf16[1,512,2048]{2,1,0:T(8,128)(2,1)}, u32[]{:S(2)}) copy-start(bf16[1,512,2048]{2,1,0:T(8,128)(2,1)} %param.53) | copy-start | bytes 6291460
  7.2 72.1 %all-gather.5.cloned.1.call-start = ((), (), s32[]{:S(2)}) async-start(), calls=%async_computation.6 | async-start | bytes 3538944 | tf_op jit(solution)/shard_map/all_gather | solution.py:145
  63.8 37.9 %copy-start.3 = (bf16[4,2048]{1,0:T(4,128)(2,1)S(1)}, bf16[4,2048]{1,0:T(4,128)(2,1)}, u32[]{:S(2)}) copy-start(bf16[4,2048]{1,0:T(4,128)(2,1)} %param.27) | copy-start | bytes 49156
  63.8 37.9 %copy-start.5 = (bf16[64,2048]{1,0:T(8,128)(2,1)S(1)}, bf16[64,2048]{1,0:T(8,128)(2,1)}, u32[]{:S(2)}) copy-start(bf16[64,2048]{1,0:T(8,128)(2,1)} %param.33) | copy-start | bytes 786436
  63.8 37.9 %copy-start.6 = (bf16[2048,64]{0,1:T(8,128)(2,1)S(1)}, bf16[2048,64]{0,1:T(8,128)(2,1)}, u32[]{:S(2)}) copy-start(bf16[2048,64]{0,1:T(8,128)(2,1)} %param.32) | copy-start | bytes 786436
  63.8 40.5 %copy-start.7 = (bf16[64,2048]{1,0:T(8,128)(2,1)S(1)}, bf16[64,2048]{1,0:T(8,128)(2,1)}, u32[]{:S(2)}) copy-start(bf16[64,2048]{1,0:T(8,128)(2,1)} %param.36) | copy-start | bytes 786436
  63.8 40.5 %copy-start.8 = (bf16[2048,64]{0,1:T(8,128)(2,1)S(1)}, bf16[2048,64]{0,1:T(8,128)(2,1)}, u32[]{:S(2)}) copy-start(bf16[2048,64]{0,1:T(8,128)(2,1)} %param.35) | copy-start | bytes 786436
  82.8 61.4 %all-to-all-start.1 = ((bf16[8,4,6144]{2,1,0:T(4,128)(2,1)}), bf16[8,4,6144]{2,1,0:T(4,128)(2,1)S(1)}, u32[]{:S(2)}, u32[]{:S(2)}) async-start(bf16[8,4,6144]{2,1,0:T(4,128)(2,1)} %reshape.104), calls=%async_computation.1 | async-start | bytes 786432 | tf_op jit(solution)/shard_map/all_to_all | solution.py:23
  100.9 99.4 %all-gather.7.cloned.1.call-start = ((), (), s32[]{:S(2)}) async-start(), calls=%async_computation.7 | async-start | bytes 1179648 | tf_op jit(solution)/shard_map/all_gather | solution.py:149
  103.5 42.2 %copy-start.9 = (f32[32,64]{1,0:T(8,128)S(1)}, f32[32,64]{1,0:T(8,128)}, u32[]{:S(2)}) copy-start(f32[32,64]{1,0:T(8,128)} %param.41) | copy-start | bytes 24580
  145.9 8.5 %copy-start.1 = (f32[4,32,64,64]{3,2,1,0:T(8,128)S(1)}, f32[4,32,64,64]{3,2,1,0:T(8,128)}, u32[]{:S(2)}) copy-start(f32[4,32,64,64]{3,2,1,0:T(8,128)} %param.28) | copy-start | bytes 6291460
  157.2 6.6 %copy-start.2 = (f32[4,32,64,64]{3,2,1,0:T(8,128)}, f32[4,32,64,64]{3,2,1,0:T(8,128)S(1)}, u32[]{:S(2)}) copy-start(f32[4,32,64,64]{3,2,1,0:T(8,128)S(1)} %multiply_add_fusion) | copy-start | bytes 6291460
  157.2 7.2 %copy-start.4 = (bf16[128,2048]{1,0:T(8,128)(2,1)S(1)}, bf16[128,2048]{1,0:T(8,128)(2,1)}, u32[]{:S(2)}) copy-start(bf16[128,2048]{1,0:T(8,128)(2,1)} %param.39) | copy-start | bytes 1572868
  157.2 7.2 %copy-start.10 = (f32[2048]{0:T(1024)S(1)}, f32[2048]{0:T(1024)}, u32[]{:S(2)}) copy-start(f32[2048]{0:T(1024)} %param.43) | copy-start | bytes 24580
  157.3 7.2 %copy-start.11 = (f32[2048]{0:T(1024)S(1)}, f32[2048]{0:T(1024)}, u32[]{:S(2)}) copy-start(f32[2048]{0:T(1024)} %param.42) | copy-start | bytes 24580
  163.9 42.5 %copy-start.12 = (f32[4,4]{1,0:T(4,128)S(1)}, f32[4,4]{1,0:T(4,128)}, u32[]{:S(2)}) copy-start(f32[4,4]{1,0:T(4,128)} %param.50) | copy-start | bytes 196
  163.9 42.7 %copy-start.17 = (s32[4,4]{1,0:T(4,128)S(1)}, s32[4,4]{1,0:T(4,128)}, u32[]{:S(2)}) copy-start(s32[4,4]{1,0:T(4,128)} %param.49) | copy-start | bytes 196
  163.9 69.6 %copy-start.13 = (f32[2048]{0:T(1024)S(1)}, f32[2048]{0:T(1024)}, u32[]{:S(2)}) copy-start(f32[2048]{0:T(1024)} %param.46) | copy-start | bytes 24580
  163.9 69.6 %copy-start.14 = (f32[2048]{0:T(1024)S(1)}, f32[2048]{0:T(1024)}, u32[]{:S(2)}) copy-start(f32[2048]{0:T(1024)} %param.45) | copy-start | bytes 24580
  202.6 30.5 %all-to-all-start.3 = ((bf16[8,4,2048]{2,1,0:T(4,128)(2,1)}), bf16[8,4,2048]{2,1,0:T(4,128)(2,1)S(1)}, u32[]{:S(2)}, u32[]{:S(2)}) async-start(bf16[8,4,2048]{2,1,0:T(4,128)(2,1)} %reshape.109), calls=%async_computation.3 | async-start | bytes 262144 | tf_op jit(solution)/shard_map/all_to_all | solution.py:23
  206.1 144.7 %all-gather.9.cloned.1.call-start = ((), (), s32[]{:S(2)}) async-start(), calls=%async_computation.8 | async-start | bytes 1131520 | tf_op jit(solution)/shard_map/all_gather | solution.py:181
  361.5 71.2 %copy-start.15 = (f32[2048]{0:T(1024)S(1)}, f32[2048]{0:T(1024)}, u32[]{:S(2)}) copy-start(f32[2048]{0:T(1024)} %param.48) | copy-start | bytes 24580
  361.5 71.2 %copy-start.16 = (f32[2048]{0:T(1024)S(1)}, f32[2048]{0:T(1024)}, u32[]{:S(2)}) copy-start(f32[2048]{0:T(1024)} %param.47) | copy-start | bytes 24580
Sparse Core Ops, SparseCore 0:
  10.4 68.8 all-gather.4
  103.5 55.7 all-gather.6
  234.3 116.4 all-gather.8

commit v2 on v1

--- a/solution.py
+++ b/solution.py
@@ -15,20 +15,19 @@
     return near, far
 
 
-def swap_features(value, axis, far):
-    return lax.all_to_all(value, axis, split_axis=1, concat_axis=0, tiled=True, axis_index_groups=far)
-
-
 def added_on_arrival(parts, axis, groups):
     got = lax.all_to_all(parts, axis, split_axis=0, concat_axis=0, tiled=True, axis_index_groups=groups)
     return jnp.sum(got.astype(jnp.float32), axis=0)
 
 
-def spread_product(rows, weight, axis, far):
-    own_rows = rows.shape[0]
-    swapped = swap_features(rows, axis, far)
-    part = jnp.dot(swapped, weight, preferred_element_type=jnp.float32).astype(jnp.bfloat16)
-    return added_on_arrival(part.reshape(-1, own_rows, weight.shape[1]), axis, far)
+def slots_of(named, own_rows, capacity):
+    owners = named.shape[0] // own_rows
+    marks = named.reshape(owners, own_rows, -1).astype(jnp.float32)
+    earlier = jnp.einsum("pr,orn->opn", jnp.tri(own_rows, k=-1, dtype=jnp.float32), marks)
+    place = jnp.arange(owners, dtype=jnp.float32)[:, None, None] * capacity + earlier
+    place = jnp.where(marks > 0, place, -1.0).reshape(owners * own_rows, -1)
+    slots = jnp.arange(owners * capacity, dtype=jnp.float32)
+    return place.T[:, None, :] == slots[None, :, None]
 
 
 def layer_norm(values_in, gain_vec, bias_vec):
@@ -142,14 +141,46 @@
     own_rows, model_width = tokens.shape
     top_count = routes.shape[1]
     near, far = near_and_far("ep")
+    blocks = len(near)
+    expert_count = lax.axis_size("ep")
+    capacity = max(2, 2 * own_rows * top_count // expert_count)
     mixer_weight = lax.all_gather(
         jnp.concatenate((receptance_matrix, key_matrix, value_matrix), axis=1),
         "ep", axis=0, tiled=True, axis_index_groups=near,
     )
-    output_weight = lax.all_gather(mixer_output_weight, "ep", axis=0, tiled=True, axis_index_groups=near)
-    receptance_rows, key_rows, value_rows = jnp.split(
-        spread_product(tokens, mixer_weight, "ep", far), 3, axis=1
-    )
+    with jax.named_scope("out_gather"):
+        output_weight = lax.all_gather(mixer_output_weight, "ep", axis=0, tiled=True)
+    share = routing_weight / jnp.sum(routing_weight, -1, keepdims=True)
+    share_high = lax.reduce_precision(share, 8, 7)
+    tail = jnp.concatenate((routes.astype(jnp.float32), share_high, share - share_high), axis=1)
+    tail = jnp.pad(tail.astype(jnp.bfloat16), ((0, 0), (0, 128 - tail.shape[1])))
+    sent = jnp.concatenate(
+        (
+            tokens.reshape(own_rows, blocks, -1),
+            jnp.broadcast_to(tail[:, None, :], (own_rows, blocks, tail.shape[1])),
+        ),
+        axis=2,
+    )
+    swapped = lax.all_to_all(sent, "ep", split_axis=1, concat_axis=0, tiled=True, axis_index_groups=far)
+    swapped = swapped.reshape(blocks * own_rows, -1)
+    features = swapped[:, : model_width // blocks]
+    tail_in = swapped[:, model_width // blocks :].astype(jnp.float32)
+    part = jnp.dot(features, mixer_weight, preferred_element_type=jnp.float32).astype(jnp.bfloat16)
+    with jax.named_scope("part_swap"):
+        projected = added_on_arrival(part.reshape(blocks, own_rows, -1), "ep", far)
+    receptance_rows, key_rows, value_rows = jnp.split(projected, 3, axis=1)
+    first_expert = lax.axis_index("ep") // NEAR * NEAR
+    experts = (first_expert + jnp.arange(NEAR)).astype(jnp.float32)
+    hits = tail_in[:, :top_count, None] == experts[None, None, :]
+    picked = slots_of(jnp.any(hits, axis=1), own_rows, capacity)
+    dispatch = picked.reshape(-1, blocks * own_rows).astype(jnp.bfloat16)
+
+    def shares_by_slot(first):
+        by_expert = jnp.sum(jnp.where(hits, tail_in[:, first : first + top_count, None], 0.0), axis=1)
+        spread = jnp.where(picked, by_expert.T[:, None, :], 0.0)
+        return spread.reshape(-1, blocks * own_rows).astype(jnp.bfloat16)
+
+    gather_high, gather_low = shares_by_slot(top_count), shares_by_slot(2 * top_count)
     mixer_result, next_state = recurrent_readout(
         tokens,
         prior_state,
@@ -169,31 +200,35 @@
         per_head_gain,
         per_head_bias,
     )
-    mixed = spread_product(mixer_result, output_weight, "ep", far)
+    mixed = jnp.dot(mixer_result, output_weight, preferred_element_type=jnp.float32)
     hidden = layer_norm(
         tokens.astype(jnp.float32) + mixed, mixer_norm_gain, mixer_norm_bias
     ).astype(jnp.bfloat16)
-    share = routing_weight / jnp.sum(routing_weight, -1, keepdims=True)
-    share_high = lax.reduce_precision(share, 8, 7)
-    share_low = share - share_high
-    tail = jnp.concatenate((routes.astype(jnp.float32), share_high, share_low), axis=1)
-    tail = jnp.pad(tail.astype(jnp.bfloat16), ((0, 0), (0, 128 - tail.shape[1])))
-    gathered = lax.all_gather(
-        jnp.concatenate((hidden, tail), axis=1), "ep", axis=0, tiled=True
-    )
-    rows_in = gathered[:, :model_width]
-    tail_in = gathered[:, model_width:].astype(jnp.float32)
-    named = tail_in[:, :top_count] == lax.axis_index("ep").astype(jnp.float32)
-    shares = tail_in[:, top_count : 2 * top_count] + tail_in[:, 2 * top_count : 3 * top_count]
-    weight_of = jnp.sum(jnp.where(named, shares, 0.0), axis=1, keepdims=True)
-    gate_val = jnp.dot(rows_in, expert_gate_weight[0], preferred_element_type=jnp.float32)
-    up_val = jnp.dot(rows_in, expert_up_weight[0], preferred_element_type=jnp.float32)
+    class_rows = lax.all_to_all(
+        jnp.broadcast_to(hidden[None], (blocks, own_rows, model_width)),
+        "ep", 0, 0, tiled=True, axis_index_groups=far,
+    ).reshape(blocks * own_rows, model_width)
+    outgoing = jnp.dot(dispatch, class_rows, preferred_element_type=jnp.float32).astype(jnp.bfloat16)
+    arrived = lax.all_to_all(
+        outgoing.reshape(NEAR, -1, model_width), "ep", 0, 0, tiled=True, axis_index_groups=near
+    )
+    flat_in = arrived.reshape(-1, model_width)
+    gate_val = jnp.dot(flat_in, expert_gate_weight[0], preferred_element_type=jnp.float32)
+    up_val = jnp.dot(flat_in, expert_up_weight[0], preferred_element_type=jnp.float32)
     inner = (jax.nn.silu(gate_val) * up_val).astype(jnp.bfloat16)
-    produced = jnp.dot(inner, expert_down_weight[0], preferred_element_type=jnp.float32)
-    given = (produced * weight_of).astype(jnp.bfloat16)
-    by_class = given.reshape(-1, NEAR, own_rows, model_width).swapaxes(0, 1)
-    block_sum = added_on_arrival(by_class, "ep", near).astype(jnp.bfloat16)
-    combined = added_on_arrival(block_sum, "ep", far)
+    produced = jnp.dot(inner, expert_down_weight[0], preferred_element_type=jnp.float32).astype(
+        jnp.bfloat16
+    )
+    returned = lax.all_to_all(
+        produced.reshape(NEAR, -1, model_width), "ep", 0, 0, tiled=True, axis_index_groups=near
+    ).reshape(-1, model_width)
+    over_slots = (((0,), (0,)), ((), ()))
+    block_sum = lax.dot_general(
+        gather_high, returned, over_slots, preferred_element_type=jnp.float32
+    ) + lax.dot_general(gather_low, returned, over_slots, preferred_element_type=jnp.float32)
+    combined = added_on_arrival(
+        block_sum.astype(jnp.bfloat16).reshape(blocks, own_rows, model_width), "ep", far
+    )
     result = layer_norm(
         hidden.astype(jnp.float32) + combined, expert_norm_gain, expert_norm_bias
     ).astype(jnp.bfloat16)

time: 441 us -> 380 us (0.86)
  blocking collectives: 158 us -> 108 us
  waiting for transfers between devices: 198 us -> 174 us
  starting transfers between devices: 22.1 us -> 35.5 us
    all_gather x2 -> x1, waiting for transfers between devices: 117 us -> 65.4 us  [body(): lax.all_gather(mixer_output_weight, 'ep', axis=0, tiled=True)]
    all_to_all x0 -> x2, waiting for transfers between devices: none -> 42 us  [the longest x1 27.1 us: body(): lax.all_to_all(jnp.broadcast_to(hidden[None], (blocks, own_rows, model_wi...]
    all_to_all x2 -> x1, blocking collectives: 70.1 us -> 33.1 us  [added_on_arrival(): lax.all_to_all(parts, axis, split_axis=0, concat_axis=0, tiled=True, axis...]
    all_to_all x0 -> x2, starting transfers between devices: none -> 16.5 us  [the longest x1 12.8 us: body(): lax.all_to_all(jnp.broadcast_to(hidden[None], (blocks, own_rows, model_wi...]
    all_to_all x2, blocking collectives: 88.4 us -> 74.7 us  [the longest x1 54.3 us: body(): lax.all_to_all(sent, 'ep', split_axis=1, concat_axis=0, tiled=True, axis_...]
    all_to_all x2 -> x1, waiting for transfers between devices: 64.9 us -> 53.6 us  [added_on_arrival(): lax.all_to_all(parts, axis, split_axis=0, concat_axis=0, tiled=True, axis...]
    all_to_all x2 -> x1, starting transfers between devices: 21.7 us -> 18.9 us  [added_on_arrival(): lax.all_to_all(parts, axis, split_axis=0, concat_axis=0, tiled=True, axis...]
    dot_general x4 -> x8, matrix products: 8.58 us -> 10.5 us  [the longest x1 4.79 us: body(): jnp.dot(mixer_result, output_weight, preferred_element_type=jnp.float32)]
  transfers between devices with their start and end apart: 5 -> 5, of which waited for: 4 -> 5; matrix products, arithmetic and copies ran while one was open for 6% -> 8% of each run, Pallas kernels for 0% -> 0%
where the time goes in v2:
time: 380 us; the launch traced here: 379 us
  waiting for transfers between devices  174 us (46%)
  blocking collectives  108 us (28%)
  starting transfers between devices  35.5 us (9%)
  matrix products  31.6 us (8%)
  between operations  14.4 us (4%)
  other arithmetic  10.3 us (3%)
  local copies, waits for them, and re-layouts  5.1 us (1%)
    all_gather x1, waiting for transfers between devices, body(): lax.all_gather(mixer_output_weight, 'ep', axis=0, tiled=True)  65.4 us
    all_to_all x1, blocking collectives, body(): lax.all_to_all(sent, 'ep', split_axis=1, concat_axis=0, tiled=True, axis_...  54.3 us
    all_to_all x1, waiting for transfers between devices, added_on_arrival(): lax.all_to_all(parts, axis, split_axis=0, concat_axis=0, tiled=True, axis...  53.6 us
    all_to_all x1, blocking collectives, added_on_arrival(): lax.all_to_all(parts, axis, split_axis=0, concat_axis=0, tiled=True, axis...  33.1 us
    all_to_all x1, waiting for transfers between devices, body(): lax.all_to_all(jnp.broadcast_to(hidden[None], (blocks, own_rows, model_wi...  27.1 us
    all_to_all x1, blocking collectives, body(): lax.all_to_all(outgoing.reshape(NEAR, -1, model_width), 'ep', 0, 0, tiled...  20.5 us
    all_to_all x1, starting transfers between devices, added_on_arrival(): lax.all_to_all(parts, axis, split_axis=0, concat_axis=0, tiled=True, axis...  18.9 us
    all_to_all x1, waiting for transfers between devices, body(): lax.all_to_all(produced.reshape(NEAR, -1, model_width), 'ep', 0, 0, tiled...  14.9 us
  transfers between devices with their start and end apart: 5, of which 5 were waited for; matrix products, arithmetic and copies ran while one was open for 8% of the time, Pallas kernels for 0%

profile of v2, /device:TPU:38, one launch (start us, length us, event | category | flops | bytes accessed | tf_op | source)
XLA Modules:
  0.0 379.1 jit_solution(17324076331513512559)
XLA Ops:
  7.3 2.0 pad_maximum_fusion
  9.4 0.7 all-gather.5.cloned.1.call-update
  10.1 0.8 reduce_sum.117
  10.9 0.8 reduce-precision_convert_fusion
  11.7 0.7 convert_convert_fusion
  12.5 0.7 pad_maximum_fusion.1
  13.2 54.3 %all_to_all.40 = bf16[4,8,384]{2,0,1:T(4,128)(2,1)S(1)} all-to-all(bf16[4,8,384]{2,0,1:T(4,128)(2,1)S(1)} %pad_maximum_fusion.1), channel_id=1, replica_groups={{0,8,16,24,32,40,48,56},{1,9,17,25,33,41,49,57},{2,10,18,26,34,42,50,58..., dimensions={1} | all-to-all | bytes 49152 | tf_op jit(solution)/shard_map/all_to_all | solution.py:164
  67.5 12.7 %all-gather.3.cloned.1.call-done = bf16[256,6144]{1,0:T(8,128)(2,1)} async-done(((bf16[32,6144]{1,0:T(8,128)(2,1)}), bf16[256,6144]{1,0:T(8,128)(2,1)}) %all-gather.3.cloned.1.call-update) | async-done | bytes 3145744 | tf_op jit(solution)/shard_map/all_gather | solution.py:147
  80.2 2.5 convolution_convert_fusion
  82.7 0.9 reshape.193
  83.6 18.9 %all-to-all-start.1 = ((bf16[8,4,6144]{2,1,0:T(4,128)(2,1)}), bf16[8,4,6144]{2,1,0:T(4,128)(2,1)S(1)}, u32[]{:S(2)}, u32[]{:S(2)}) async-start(bf16[8,4,6144]{2,1,0:T(4,128)(2,1)} %reshape.193), calls=%async_computation.1 | async-start | bytes 786432 | tf_op jit(solution)/shard_map/part_swap/all_to_all | solution.py:19
  102.5 1.3 fusion.6
  104.0 1.5 fusion.40
  105.8 53.6 %all-to-all-done.1 = bf16[8,4,6144]{2,1,0:T(4,128)(2,1)S(1)} async-done(((bf16[8,4,6144]{2,1,0:T(4,128)(2,1)}), bf16[8,4,6144]{2,1,0:T(4,128)(2,1)S(1)}, u32[]{:S(2)}, u32[]{:S(2)}) %all-to-all-start.1) | async-done | bytes 393248 | tf_op jit(solution)/shard_map/part_swap/all_to_all | solution.py:19
  160.3 8.5 %fusion.76 = f32[4,32,1,64]{3,2,1,0:T(1,128)S(1)} fusion(f32[4,32,64,1]{2,3,1,0:T(1,128)S(1)} %bitcast.86, f32[4,32,64,64]{3,2,1,0:T(8,128)} %param.28), kind=kOutput, calls=%fused_computation.123 | convolution fusion | flops 6291456 | bytes 2162688 | tf_op jit(solution)/shard_map/nhvk,nhk->nhv/dot_general | solution.py:89
  168.8 2.8 multiply_add_fusion
  171.6 2.0 copy-done.2
  173.6 6.6 %fusion.77 = f32[4,32,1,64]{3,2,1,0:T(1,128)S(1)} fusion(f32[4,32,64,64]{3,2,1,0:T(8,128)S(1)} %multiply_add_fusion, f32[4,32,64,1]{2,3,1,0:T(1,128)S(1)} %bitcast.85), kind=kOutput, calls=%fused_computation.124 | convolution fusion | flops 6291456 | bytes 2162688 | tf_op jit(solution)/shard_map/nhvk,nhk->nhv/dot_general | solution.py:95
  180.9 65.4 %all-gather.5.cloned.1.call-done = bf16[2048,2048]{1,0:T(8,128)(2,1)} async-done(((bf16[32,2048]{1,0:T(8,128)(2,1)}), bf16[2048,2048]{1,0:T(8,128)(2,1)}) %all-gather.5.cloned.1.call-update) | async-done | bytes 8388624 | tf_op jit(solution)/shard_map/out_gather/all_gather | solution.py:152
  246.2 4.8 %fusion.75 = (f32[4]{0:T(128)S(1)}, f32[4,2048]{1,0:T(4,128)S(1)}) fusion(bf16[2048,2048]{1,0:T(8,128)(2,1)} %all-gather.5.cloned.1.call-done, bf16[4,128]{1,0:T(4,128)(2,1)S(1)} %fusion.28, bf16[128,2048]{1,0:T(8,128)(2,1)S(1)} %copy-done.3, f32[4,2048]{1,0:T(4,128)S(1)} %mul.200, f32[4,2048]{1,0:T(4,128)S(1)} %reshape.197, f32[2048]{0:T(1024)S(1)} %copy-done.12, ...), kind=kOutput, calls=%fused_computation.122 | convolution fusion | flops 35725308 | bytes 9077776 | tf_op jit(solution)/shard_map/dot_general | solution.py:203
  251.4 0.7 broadcast_in_dim.50
  252.0 12.8 %all-to-all-start.2 = ((bf16[8,4,2048]{2,1,0:T(4,128)(2,1)}), bf16[8,4,2048]{2,1,0:T(4,128)(2,1)S(1)}, u32[]{:S(2)}, u32[]{:S(2)}) async-start(bf16[8,4,2048]{2,1,0:T(4,128)(2,1)} %broadcast_in_dim.50), calls=%async_computation.2 | async-start | bytes 262144 | tf_op jit(solution)/shard_map/all_to_all | solution.py:207
  265.5 27.1 %all-to-all-done.2 = bf16[8,4,2048]{2,1,0:T(4,128)(2,1)S(1)} async-done(((bf16[8,4,2048]{2,1,0:T(4,128)(2,1)}), bf16[8,4,2048]{2,1,0:T(4,128)(2,1)S(1)}, u32[]{:S(2)}, u32[]{:S(2)}) %all-to-all-start.2) | async-done | bytes 131104 | tf_op jit(solution)/shard_map/all_to_all | solution.py:207
  292.6 0.3 convolution_convert_fusion.2
  292.9 20.5 %all_to_all.41 = bf16[8,16,2048]{2,1,0:T(8,128)(2,1)S(1)} all-to-all(bf16[8,16,2048]{2,1,0:T(8,128)(2,1)S(1)} %bitcast.79), channel_id=1, replica_groups={{0,1,2,3,4,5,6,7},{8,9,10,11,12,13,14,15},{16,17,18,19,20,21,22,23},{24..., dimensions={0} | all-to-all | bytes 1048576 | tf_op jit(solution)/shard_map/all_to_all | solution.py:212
  313.3 2.0 fusion.12
  315.4 3.2 convolution_convert_fusion.1
  318.6 3.7 all-to-all-start.4
  322.6 14.9 %all-to-all-done.4 = bf16[8,16,2048]{2,1,0:T(8,128)(2,1)S(1)} async-done(((bf16[8,16,2048]{2,1,0:T(8,128)(2,1)}), bf16[8,16,2048]{2,1,0:T(8,128)(2,1)S(1)}, u32[]{:S(2)}, u32[]{:S(2)}) %all-to-all-start.4) | async-done | bytes 524320 | tf_op jit(solution)/shard_map/all_to_all | solution.py:222
  337.7 0.3 fusion.2
  338.0 33.1 %all_to_all.42 = bf16[8,4,2048]{2,1,0:T(4,128)(2,1)S(1)} all-to-all(bf16[8,4,2048]{2,1,0:T(4,128)(2,1)S(1)} %reshape.204), channel_id=1, replica_groups={{0,8,16,24,32,40,48,56},{1,9,17,25,33,41,49,57},{2,10,18,26,34,42,50,58..., dimensions={0} | all-to-all | bytes 262144 | tf_op jit(solution)/shard_map/all_to_all | solution.py:19
  371.6 0.7 add_convert_fusion
  (87 shorter events, 4.3 us)
Async XLA Ops:
  7.2 308.2 %copy-start = (bf16[1,512,2048]{2,1,0:T(8,128)(2,1)S(1)}, bf16[1,512,2048]{2,1,0:T(8,128)(2,1)}, u32[]{:S(2)}) copy-start(bf16[1,512,2048]{2,1,0:T(8,128)(2,1)} %param.53) | copy-start | bytes 6291460
  7.2 95.3 %copy-start.5 = (bf16[4,2048]{1,0:T(4,128)(2,1)S(1)}, bf16[4,2048]{1,0:T(4,128)(2,1)}, u32[]{:S(2)}) copy-start(bf16[4,2048]{1,0:T(4,128)(2,1)} %param.27) | copy-start | bytes 49156
  7.2 95.3 %copy-start.6 = (bf16[64,2048]{1,0:T(8,128)(2,1)S(1)}, bf16[64,2048]{1,0:T(8,128)(2,1)}, u32[]{:S(2)}) copy-start(bf16[64,2048]{1,0:T(8,128)(2,1)} %param.36) | copy-start | bytes 786436
  7.2 95.3 %copy-start.10 = (f32[2048]{0:T(1024)S(1)}, f32[2048]{0:T(1024)}, u32[]{:S(2)}) copy-start(f32[2048]{0:T(1024)} %param.37) | copy-start | bytes 24580
  7.2 96.8 %copy-start.11 = (f32[2048]{0:T(1024)S(1)}, f32[2048]{0:T(1024)}, u32[]{:S(2)}) copy-start(f32[2048]{0:T(1024)} %param.34) | copy-start | bytes 24580
  7.2 98.3 %copy-start.4 = (bf16[2048,128]{1,0:T(8,128)(2,1)S(1)}, bf16[2048,128]{1,0:T(8,128)(2,1)}, u32[]{:S(2)}) copy-start(bf16[2048,128]{1,0:T(8,128)(2,1)} %param.38) | copy-start | bytes 1572868
  7.2 72.9 %all-gather.3.cloned.1.call-start = ((), (), s32[]{:S(2)}) async-start(), calls=%async_computation.6 | async-start | bytes 3538944 | tf_op jit(solution)/shard_map/all_gather | solution.py:147
  9.3 150.2 %copy-start.16 = (f32[2048]{0:T(1024)S(1)}, f32[2048]{0:T(1024)}, u32[]{:S(2)}) copy-start(f32[2048]{0:T(1024)} %param.40) | copy-start | bytes 24580
  9.3 236.9 %all-gather.5.cloned.1.call-start = ((), (), s32[]{:S(2)}) async-start(), calls=%async_computation.7 | async-start | bytes 8519680 | tf_op jit(solution)/shard_map/out_gather/all_gather | solution.py:152
  83.6 75.7 %all-to-all-start.1 = ((bf16[8,4,6144]{2,1,0:T(4,128)(2,1)}), bf16[8,4,6144]{2,1,0:T(4,128)(2,1)S(1)}, u32[]{:S(2)}, u32[]{:S(2)}) async-start(bf16[8,4,6144]{2,1,0:T(4,128)(2,1)} %reshape.193), calls=%async_computation.1 | async-start | bytes 786432 | tf_op jit(solution)/shard_map/part_swap/all_to_all | solution.py:19
  160.1 8.7 %copy-start.1 = (f32[4,32,64,64]{3,2,1,0:T(8,128)S(1)}, f32[4,32,64,64]{3,2,1,0:T(8,128)}, u32[]{:S(2)}) copy-start(f32[4,32,64,64]{3,2,1,0:T(8,128)} %param.28) | copy-start | bytes 6291460
  171.5 2.0 copy-start.2
  171.5 9.1 %copy-start.9 = (f32[32,64]{1,0:T(8,128)S(1)}, f32[32,64]{1,0:T(8,128)}, u32[]{:S(2)}) copy-start(f32[32,64]{1,0:T(8,128)} %param.41) | copy-start | bytes 24580
  171.6 74.7 %copy-start.3 = (bf16[128,2048]{1,0:T(8,128)(2,1)S(1)}, bf16[128,2048]{1,0:T(8,128)(2,1)}, u32[]{:S(2)}) copy-start(bf16[128,2048]{1,0:T(8,128)(2,1)} %param.39) | copy-start | bytes 1572868
  171.6 74.7 %copy-start.12 = (f32[2048]{0:T(1024)S(1)}, f32[2048]{0:T(1024)}, u32[]{:S(2)}) copy-start(f32[2048]{0:T(1024)} %param.43) | copy-start | bytes 24580
  171.6 74.7 %copy-start.13 = (f32[2048]{0:T(1024)S(1)}, f32[2048]{0:T(1024)}, u32[]{:S(2)}) copy-start(f32[2048]{0:T(1024)} %param.42) | copy-start | bytes 24580
  180.8 70.4 %copy-start.7 = (f32[2048]{0:T(1024)S(1)}, f32[2048]{0:T(1024)}, u32[]{:S(2)}) copy-start(f32[2048]{0:T(1024)} %param.46) | copy-start | bytes 24580
  180.8 70.4 %copy-start.8 = (f32[2048]{0:T(1024)S(1)}, f32[2048]{0:T(1024)}, u32[]{:S(2)}) copy-start(f32[2048]{0:T(1024)} %param.45) | copy-start | bytes 24580
  252.0 40.5 %all-to-all-start.2 = ((bf16[8,4,2048]{2,1,0:T(4,128)(2,1)}), bf16[8,4,2048]{2,1,0:T(4,128)(2,1)S(1)}, u32[]{:S(2)}, u32[]{:S(2)}) async-start(bf16[8,4,2048]{2,1,0:T(4,128)(2,1)} %broadcast_in_dim.50), calls=%async_computation.2 | async-start | bytes 262144 | tf_op jit(solution)/shard_map/all_to_all | solution.py:207
  315.4 56.2 %copy-start.14 = (f32[2048]{0:T(1024)S(1)}, f32[2048]{0:T(1024)}, u32[]{:S(2)}) copy-start(f32[2048]{0:T(1024)} %param.48) | copy-start | bytes 24580
  315.4 56.2 %copy-start.15 = (f32[2048]{0:T(1024)S(1)}, f32[2048]{0:T(1024)}, u32[]{:S(2)}) copy-start(f32[2048]{0:T(1024)} %param.47) | copy-start | bytes 24580
  318.6 18.8 %all-to-all-start.4 = ((bf16[8,16,2048]{2,1,0:T(8,128)(2,1)}), bf16[8,16,2048]{2,1,0:T(8,128)(2,1)S(1)}, u32[]{:S(2)}, u32[]{:S(2)}) async-start(bf16[8,16,2048]{2,1,0:T(8,128)(2,1)} %bitcast.22), calls=%async_computation.4 | async-start | bytes 1048576 | tf_op jit(solution)/shard_map/all_to_all | solution.py:222
Sparse Core Ops, SparseCore 0:
  10.5 69.6 all-gather.2
  82.0 164.1 all-gather.4

commit v3 on v2

--- a/solution.py
+++ b/solution.py
@@ -148,8 +148,7 @@
         jnp.concatenate((receptance_matrix, key_matrix, value_matrix), axis=1),
         "ep", axis=0, tiled=True, axis_index_groups=near,
     )
-    with jax.named_scope("out_gather"):
-        output_weight = lax.all_gather(mixer_output_weight, "ep", axis=0, tiled=True)
+    output_weight = lax.all_gather(mixer_output_weight, "ep", axis=0, tiled=True, axis_index_groups=far)
     share = routing_weight / jnp.sum(routing_weight, -1, keepdims=True)
     share_high = lax.reduce_precision(share, 8, 7)
     tail = jnp.concatenate((routes.astype(jnp.float32), share_high, share - share_high), axis=1)
@@ -166,8 +165,7 @@
     features = swapped[:, : model_width // blocks]
     tail_in = swapped[:, model_width // blocks :].astype(jnp.float32)
     part = jnp.dot(features, mixer_weight, preferred_element_type=jnp.float32).astype(jnp.bfloat16)
-    with jax.named_scope("part_swap"):
-        projected = added_on_arrival(part.reshape(blocks, own_rows, -1), "ep", far)
+    projected = added_on_arrival(part.reshape(blocks, own_rows, -1), "ep", far)
     receptance_rows, key_rows, value_rows = jnp.split(projected, 3, axis=1)
     first_expert = lax.axis_index("ep") // NEAR * NEAR
     experts = (first_expert + jnp.arange(NEAR)).astype(jnp.float32)
@@ -200,7 +198,15 @@
         per_head_gain,
         per_head_bias,
     )
-    mixed = jnp.dot(mixer_result, output_weight, preferred_element_type=jnp.float32)
+    by_holder = mixer_result.reshape(own_rows, blocks, NEAR, -1).swapaxes(1, 2)
+    channels = lax.all_to_all(
+        by_holder.reshape(own_rows, NEAR, -1),
+        "ep", split_axis=1, concat_axis=0, tiled=True, axis_index_groups=near,
+    ).reshape(NEAR * own_rows, -1)
+    mixed_part = jnp.dot(channels, output_weight, preferred_element_type=jnp.float32)
+    mixed = added_on_arrival(
+        mixed_part.astype(jnp.bfloat16).reshape(NEAR, own_rows, model_width), "ep", near
+    )
     hidden = layer_norm(
         tokens.astype(jnp.float32) + mixed, mixer_norm_gain, mixer_norm_bias
     ).astype(jnp.bfloat16)

time: 380 us -> 338 us (0.89)
  waiting for transfers between devices: 174 us -> 111 us
  blocking collectives: 108 us -> 122 us
  starting transfers between devices: 35.5 us -> 42.2 us
    all_gather x1, waiting for transfers between devices: 65.4 us -> 5.39 us  [body(): lax.all_gather(mixer_output_weight, 'ep', axis=0, tiled=True, axis_index_...]
    all_to_all x0 -> x1, blocking collectives: none -> 16.8 us  [body(): lax.all_to_all(by_holder.reshape(own_rows, NEAR, -1), 'ep', split_axis=1,...]
    all_to_all x1 -> x2, starting transfers between devices: 18.9 us -> 26.3 us  [added_on_arrival(): lax.all_to_all(parts, axis, split_axis=0, concat_axis=0, tiled=True, axis...]
    all_to_all x1 -> x2, waiting for transfers between devices: 53.6 us -> 48.9 us  [added_on_arrival(): lax.all_to_all(parts, axis, split_axis=0, concat_axis=0, tiled=True, axis...]
  transfers between devices with their start and end apart: 5 -> 6, of which waited for: 5 -> 6; matrix products, arithmetic and copies ran while one was open for 8% -> 9% of each run, Pallas kernels for 0% -> 0%
where the time goes in v3:
time: 338 us; the launch traced here: 337 us
  blocking collectives  122 us (36%)
  waiting for transfers between devices  111 us (33%)
  starting transfers between devices  42.2 us (12%)
  matrix products  30.3 us (9%)
  between operations  15.9 us (5%)
  other arithmetic  11.7 us (3%)
  local copies, waits for them, and re-layouts  4.09 us (1%)
    all_to_all x1, blocking collectives, body(): lax.all_to_all(sent, 'ep', split_axis=1, concat_axis=0, tiled=True, axis_...  54.2 us
    all_to_all x2, waiting for transfers between devices, added_on_arrival(): lax.all_to_all(parts, axis, split_axis=0, concat_axis=0, tiled=True, axis...  48.9 us
    all_to_all x1, blocking collectives, added_on_arrival(): lax.all_to_all(parts, axis, split_axis=0, concat_axis=0, tiled=True, axis...  32.2 us
    all_to_all x1, waiting for transfers between devices, body(): lax.all_to_all(jnp.broadcast_to(hidden[None], (blocks, own_rows, model_wi...  28.2 us
    all_to_all x2, starting transfers between devices, added_on_arrival(): lax.all_to_all(parts, axis, split_axis=0, concat_axis=0, tiled=True, axis...  26.3 us
    all_to_all x1, blocking collectives, body(): lax.all_to_all(outgoing.reshape(NEAR, -1, model_width), 'ep', 0, 0, tiled...  18.5 us
    all_to_all x1, blocking collectives, body(): lax.all_to_all(by_holder.reshape(own_rows, NEAR, -1), 'ep', split_axis=1,...  16.8 us
    all_to_all x1, waiting for transfers between devices, body(): lax.all_to_all(produced.reshape(NEAR, -1, model_width), 'ep', 0, 0, tiled...  14.9 us
  transfers between devices with their start and end apart: 6, of which 6 were waited for; matrix products, arithmetic and copies ran while one was open for 9% of the time, Pallas kernels for 0%

profile of v3, /device:TPU:38, one launch (start us, length us, event | category | flops | bytes accessed | tf_op | source)
XLA Modules:
  0.0 337.2 jit_solution(14190382681940183096)
XLA Ops:
  8.2 2.0 pad_maximum_fusion
  10.2 0.8 reduce_sum.126
  11.0 0.8 reduce-precision_convert_fusion
  11.8 0.7 convert_convert_fusion
  12.5 0.7 pad_maximum_fusion.1
  13.3 54.2 %all_to_all.60 = bf16[4,8,384]{2,0,1:T(4,128)(2,1)S(1)} all-to-all(bf16[4,8,384]{2,0,1:T(4,128)(2,1)S(1)} %pad_maximum_fusion.1), channel_id=1, replica_groups={{0,8,16,24,32,40,48,56},{1,9,17,25,33,41,49,57},{2,10,18,26,34,42,50,58..., dimensions={1} | all-to-all | bytes 49152 | tf_op jit(solution)/shard_map/all_to_all | solution.py:163
  67.5 13.3 %all-gather.3.cloned.1.call-done = bf16[256,6144]{1,0:T(8,128)(2,1)} async-done(((bf16[32,6144]{1,0:T(8,128)(2,1)}), bf16[256,6144]{1,0:T(8,128)(2,1)}) %all-gather.3.cloned.1.call-update) | async-done | bytes 3145744 | tf_op jit(solution)/shard_map/all_gather | solution.py:147
  80.9 2.5 convolution_convert_fusion
  83.4 0.9 reshape.206
  84.3 18.8 %all-to-all-start.1 = ((bf16[8,4,6144]{2,1,0:T(4,128)(2,1)}), bf16[8,4,6144]{2,1,0:T(4,128)(2,1)S(1)}, u32[]{:S(2)}, u32[]{:S(2)}) async-start(bf16[8,4,6144]{2,1,0:T(4,128)(2,1)} %reshape.206), calls=%async_computation.1 | async-start | bytes 786432 | tf_op jit(solution)/shard_map/all_to_all | solution.py:19
  104.3 1.4 fusion.40
  105.8 42.1 %all-to-all-done.1 = bf16[8,4,6144]{2,1,0:T(4,128)(2,1)S(1)} async-done(((bf16[8,4,6144]{2,1,0:T(4,128)(2,1)}), bf16[8,4,6144]{2,1,0:T(4,128)(2,1)S(1)}, u32[]{:S(2)}, u32[]{:S(2)}) %all-to-all-start.1) | async-done | bytes 393248 | tf_op jit(solution)/shard_map/all_to_all | solution.py:19
  148.6 8.5 %fusion.71 = f32[4,32,1,64]{3,2,1,0:T(1,128)S(1)} fusion(f32[4,32,64,1]{2,3,1,0:T(1,128)S(1)} %bitcast.96, f32[4,32,64,64]{3,2,1,0:T(8,128)} %param.28), kind=kOutput, calls=%fused_computation.121 | convolution fusion | flops 6291456 | bytes 2162688 | tf_op jit(solution)/shard_map/nhvk,nhk->nhv/dot_general | solution.py:89
  157.2 4.0 %multiply_add_fusion = f32[4,32,64,64]{3,2,1,0:T(8,128)} fusion(f32[4,32,64,64]{3,2,1,0:T(8,128)S(1)} %copy-done.1, f32[4,32,64]{2,1,0:T(8,128)S(1)} %mul.188, f32[4,32,64]{2,1,0:T(8,128)S(1)} %mul.183, f32[4,32,64]{2,1,0:T(8,128)S(1)} %get-tuple-element.4, f32[4,32,64]{2,1,0:T(8,128)S(1)} %bitcast.94, f32[4,32,64]{2,1,0:T(8,128)S(1)} %mul.173), kind=kLoop, calls=%fused_computation.2 | loop fusion | flops 2621440 | bytes 4358144 | tf_op jit(solution)/shard_map/add | solution.py:91
  161.4 8.3 %fusion.72 = f32[4,32,1,64]{3,2,1,0:T(1,128)S(1)} fusion(f32[4,32,64,64]{3,2,1,0:T(8,128)} %multiply_add_fusion, f32[4,32,64,1]{2,3,1,0:T(1,128)S(1)} %bitcast.95), kind=kOutput, calls=%fused_computation.122 | convolution fusion | flops 6291456 | bytes 2162688 | tf_op jit(solution)/shard_map/nhvk,nhk->nhv/dot_general | solution.py:95
  170.5 1.4 fusion.8
  172.1 16.8 %all_to_all.61 = bf16[4,8,256]{2,0,1:T(4,128)(2,1)S(1)} all-to-all(bf16[4,8,256]{2,0,1:T(4,128)(2,1)S(1)} %copy.40), channel_id=1, replica_groups={{0,1,2,3,4,5,6,7},{8,9,10,11,12,13,14,15},{16,17,18,19,20,21,22,23},{24..., dimensions={1} | all-to-all | bytes 32768 | tf_op jit(solution)/shard_map/all_to_all | solution.py:202
  188.9 5.4 %all-gather.5.cloned.1.call-done = bf16[256,2048]{1,0:T(8,128)(2,1)} async-done(((bf16[32,2048]{1,0:T(8,128)(2,1)}), bf16[256,2048]{1,0:T(8,128)(2,1)}) %all-gather.5.cloned.1.call-update) | async-done | bytes 1048592 | tf_op jit(solution)/shard_map/all_gather | solution.py:151
  194.3 1.5 convolution_convert_fusion.3
  195.8 0.7 reshape.214
  196.5 7.5 %all-to-all-start.3 = ((bf16[8,4,2048]{2,1,0:T(4,128)(2,1)}), bf16[8,4,2048]{2,1,0:T(4,128)(2,1)S(1)}, u32[]{:S(2)}, u32[]{:S(2)}) async-start(bf16[8,4,2048]{2,1,0:T(4,128)(2,1)} %reshape.214), calls=%async_computation.3 | async-start | bytes 262144 | tf_op jit(solution)/shard_map/all_to_all | solution.py:19
  204.0 6.7 %all-to-all-done.3 = bf16[8,4,2048]{2,1,0:T(4,128)(2,1)S(1)} async-done(((bf16[8,4,2048]{2,1,0:T(4,128)(2,1)}), bf16[8,4,2048]{2,1,0:T(4,128)(2,1)S(1)}, u32[]{:S(2)}, u32[]{:S(2)}) %all-to-all-start.3) | async-done | bytes 131104 | tf_op jit(solution)/shard_map/all_to_all | solution.py:19
  211.3 0.7 broadcast_in_dim.50
  211.9 12.1 %all-to-all-start.4 = ((bf16[8,4,2048]{2,1,0:T(4,128)(2,1)}), bf16[8,4,2048]{2,1,0:T(4,128)(2,1)S(1)}, u32[]{:S(2)}, u32[]{:S(2)}) async-start(bf16[8,4,2048]{2,1,0:T(4,128)(2,1)} %broadcast_in_dim.50), calls=%async_computation.4 | async-start | bytes 262144 | tf_op jit(solution)/shard_map/all_to_all | solution.py:213
  224.6 28.2 %all-to-all-done.4 = bf16[8,4,2048]{2,1,0:T(4,128)(2,1)S(1)} async-done(((bf16[8,4,2048]{2,1,0:T(4,128)(2,1)}), bf16[8,4,2048]{2,1,0:T(4,128)(2,1)S(1)}, u32[]{:S(2)}, u32[]{:S(2)}) %all-to-all-start.4) | async-done | bytes 131104 | tf_op jit(solution)/shard_map/all_to_all | solution.py:213
  253.2 18.5 %all_to_all.62 = bf16[8,16,2048]{2,1,0:T(8,128)(2,1)S(1)} all-to-all(bf16[8,16,2048]{2,1,0:T(8,128)(2,1)S(1)} %bitcast.89), channel_id=1, replica_groups={{0,1,2,3,4,5,6,7},{8,9,10,11,12,13,14,15},{16,17,18,19,20,21,22,23},{24..., dimensions={0} | all-to-all | bytes 1048576 | tf_op jit(solution)/shard_map/all_to_all | solution.py:218
  271.7 2.0 fusion.12
  273.8 3.2 convolution_convert_fusion.1
  277.0 3.7 %all-to-all-start.6 = ((bf16[8,16,2048]{2,1,0:T(8,128)(2,1)}), bf16[8,16,2048]{2,1,0:T(8,128)(2,1)S(1)}, u32[]{:S(2)}, u32[]{:S(2)}) async-start(bf16[8,16,2048]{2,1,0:T(8,128)(2,1)} %bitcast.25), calls=%async_computation.6 | async-start | bytes 1048576 | tf_op jit(solution)/shard_map/all_to_all | solution.py:228
  281.0 14.9 %all-to-all-done.6 = bf16[8,16,2048]{2,1,0:T(8,128)(2,1)S(1)} async-done(((bf16[8,16,2048]{2,1,0:T(8,128)(2,1)}), bf16[8,16,2048]{2,1,0:T(8,128)(2,1)S(1)}, u32[]{:S(2)}, u32[]{:S(2)}) %all-to-all-start.6) | async-done | bytes 524320 | tf_op jit(solution)/shard_map/all_to_all | solution.py:228
  296.4 32.2 %all_to_all.63 = bf16[8,4,2048]{2,1,0:T(4,128)(2,1)S(1)} all-to-all(bf16[8,4,2048]{2,1,0:T(4,128)(2,1)S(1)} %reshape.221), channel_id=1, replica_groups={{0,8,16,24,32,40,48,56},{1,9,17,25,33,41,49,57},{2,10,18,26,34,42,50,58..., dimensions={0} | all-to-all | bytes 262144 | tf_op jit(solution)/shard_map/all_to_all | solution.py:19
  329.0 0.7 add_convert_fusion
  (98 shorter events, 5.9 us)
Async XLA Ops:
  8.0 265.7 %copy-start = (bf16[1,512,2048]{2,1,0:T(8,128)(2,1)S(1)}, bf16[1,512,2048]{2,1,0:T(8,128)(2,1)}, u32[]{:S(2)}) copy-start(bf16[1,512,2048]{2,1,0:T(8,128)(2,1)} %param.53) | copy-start | bytes 6291460
  8.1 95.7 %copy-start.2 = (bf16[4,2048]{1,0:T(4,128)(2,1)S(1)}, bf16[4,2048]{1,0:T(4,128)(2,1)}, u32[]{:S(2)}) copy-start(bf16[4,2048]{1,0:T(4,128)(2,1)} %param.27) | copy-start | bytes 49156
  8.1 95.7 %copy-start.5 = (bf16[2048,64]{0,1:T(8,128)(2,1)S(1)}, bf16[2048,64]{0,1:T(8,128)(2,1)}, u32[]{:S(2)}) copy-start(bf16[2048,64]{0,1:T(8,128)(2,1)} %param.35) | copy-start | bytes 786436
  8.1 95.7 %copy-start.4 = (bf16[64,2048]{1,0:T(8,128)(2,1)S(1)}, bf16[64,2048]{1,0:T(8,128)(2,1)}, u32[]{:S(2)}) copy-start(bf16[64,2048]{1,0:T(8,128)(2,1)} %param.36) | copy-start | bytes 786436
  8.1 95.7 %copy-start.8 = (f32[2048]{0:T(1024)S(1)}, f32[2048]{0:T(1024)}, u32[]{:S(2)}) copy-start(f32[2048]{0:T(1024)} %param.37) | copy-start | bytes 24580
  8.1 96.2 %copy-start.6 = (bf16[64,2048]{1,0:T(8,128)(2,1)S(1)}, bf16[64,2048]{1,0:T(8,128)(2,1)}, u32[]{:S(2)}) copy-start(bf16[64,2048]{1,0:T(8,128)(2,1)} %param.33) | copy-start | bytes 786436
  8.1 96.2 %copy-start.9 = (f32[2048]{0:T(1024)S(1)}, f32[2048]{0:T(1024)}, u32[]{:S(2)}) copy-start(f32[2048]{0:T(1024)} %param.34) | copy-start | bytes 24580
  8.1 140.0 %copy-start.12 = (f32[2048]{0:T(1024)S(1)}, f32[2048]{0:T(1024)}, u32[]{:S(2)}) copy-start(f32[2048]{0:T(1024)} %param.40) | copy-start | bytes 24580
  8.1 72.7 %all-gather.3.cloned.1.call-start = ((), (), s32[]{:S(2)}) async-start(), calls=%async_computation.8 | async-start | bytes 3538944 | tf_op jit(solution)/shard_map/all_gather | solution.py:147
  84.3 63.6 %all-to-all-start.1 = ((bf16[8,4,6144]{2,1,0:T(4,128)(2,1)}), bf16[8,4,6144]{2,1,0:T(4,128)(2,1)S(1)}, u32[]{:S(2)}, u32[]{:S(2)}) async-start(bf16[8,4,6144]{2,1,0:T(4,128)(2,1)} %reshape.206), calls=%async_computation.1 | async-start | bytes 786432 | tf_op jit(solution)/shard_map/all_to_all | solution.py:19
  103.1 91.2 %all-gather.5.cloned.1.call-start = ((), (), s32[]{:S(2)}) async-start(), calls=%async_computation.9 | async-start | bytes 1179648 | tf_op jit(solution)/shard_map/all_gather | solution.py:151
  148.5 8.6 %copy-start.1 = (f32[4,32,64,64]{3,2,1,0:T(8,128)S(1)}, f32[4,32,64,64]{3,2,1,0:T(8,128)}, u32[]{:S(2)}) copy-start(f32[4,32,64,64]{3,2,1,0:T(8,128)} %param.28) | copy-start | bytes 6291460
  161.2 9.1 %copy-start.7 = (f32[32,64]{1,0:T(8,128)S(1)}, f32[32,64]{1,0:T(8,128)}, u32[]{:S(2)}) copy-start(f32[32,64]{1,0:T(8,128)} %param.41) | copy-start | bytes 24580
  161.2 9.3 %copy-start.3 = (bf16[128,2048]{1,0:T(8,128)(2,1)S(1)}, bf16[128,2048]{1,0:T(8,128)(2,1)}, u32[]{:S(2)}) copy-start(bf16[128,2048]{1,0:T(8,128)(2,1)} %param.39) | copy-start | bytes 1572868
  161.2 9.3 %copy-start.10 = (f32[2048]{0:T(1024)S(1)}, f32[2048]{0:T(1024)}, u32[]{:S(2)}) copy-start(f32[2048]{0:T(1024)} %param.43) | copy-start | bytes 24580
  161.2 9.3 %copy-start.11 = (f32[2048]{0:T(1024)S(1)}, f32[2048]{0:T(1024)}, u32[]{:S(2)}) copy-start(f32[2048]{0:T(1024)} %param.42) | copy-start | bytes 24580
  161.4 49.8 %copy-start.13 = (f32[2048]{0:T(1024)S(1)}, f32[2048]{0:T(1024)}, u32[]{:S(2)}) copy-start(f32[2048]{0:T(1024)} %param.46) | copy-start | bytes 24580
  161.4 49.8 %copy-start.14 = (f32[2048]{0:T(1024)S(1)}, f32[2048]{0:T(1024)}, u32[]{:S(2)}) copy-start(f32[2048]{0:T(1024)} %param.45) | copy-start | bytes 24580
  196.5 14.2 %all-to-all-start.3 = ((bf16[8,4,2048]{2,1,0:T(4,128)(2,1)}), bf16[8,4,2048]{2,1,0:T(4,128)(2,1)S(1)}, u32[]{:S(2)}, u32[]{:S(2)}) async-start(bf16[8,4,2048]{2,1,0:T(4,128)(2,1)} %reshape.214), calls=%async_computation.3 | async-start | bytes 262144 | tf_op jit(solution)/shard_map/all_to_all | solution.py:19
  211.9 40.9 %all-to-all-start.4 = ((bf16[8,4,2048]{2,1,0:T(4,128)(2,1)}), bf16[8,4,2048]{2,1,0:T(4,128)(2,1)S(1)}, u32[]{:S(2)}, u32[]{:S(2)}) async-start(bf16[8,4,2048]{2,1,0:T(4,128)(2,1)} %broadcast_in_dim.50), calls=%async_computation.4 | async-start | bytes 262144 | tf_op jit(solution)/shard_map/all_to_all | solution.py:213
  273.8 55.3 %copy-start.15 = (f32[2048]{0:T(1024)S(1)}, f32[2048]{0:T(1024)}, u32[]{:S(2)}) copy-start(f32[2048]{0:T(1024)} %param.48) | copy-start | bytes 24580
  273.8 55.3 %copy-start.16 = (f32[2048]{0:T(1024)S(1)}, f32[2048]{0:T(1024)}, u32[]{:S(2)}) copy-start(f32[2048]{0:T(1024)} %param.47) | copy-start | bytes 24580
  277.0 18.8 %all-to-all-start.6 = ((bf16[8,16,2048]{2,1,0:T(8,128)(2,1)}), bf16[8,16,2048]{2,1,0:T(8,128)(2,1)S(1)}, u32[]{:S(2)}, u32[]{:S(2)}) async-start(bf16[8,16,2048]{2,1,0:T(8,128)(2,1)} %bitcast.25), calls=%async_computation.6 | async-start | bytes 1048576 | tf_op jit(solution)/shard_map/all_to_all | solution.py:228
Sparse Core Ops, SparseCore 0:
  11.3 69.4 all-gather.2
Sparse Core Ops, SparseCore 1:
  105.4 88.8 all-gather.4
